TPU v7x, 32 devices: a whole 2x2x4 slice. The times are simulated.
32 devices in a mesh: sp: 8 (over z, y), dp: 4 (over x, core).
Axes of the slice: x: 2, y: 2, z: 4, core: 2. Of those that a mesh axis runs over, the one named last changes fastest.
Arguments:
- query_nope: bfloat16 [4, 2048, 16, 128], P('dp', 'sp'), may hold values from -6 to 6
- query_rope: bfloat16 [4, 2048, 16, 64], P('dp', 'sp'), may hold values from -160 to 160
- latent: bfloat16 [4, 2048, 256], P('dp', 'sp'), may hold values from -6 to 6
- key_rope: bfloat16 [4, 2048, 64], P('dp', 'sp'), may hold values from -4 to 4
- resid: bfloat16 [4, 2048, 2048], P('dp', 'sp'), may hold values from -6 to 6
- latent_gain: float32 [256], replicated, may hold values from 0.1 to 1.9
- key_up: bfloat16 [256, 2048], P(None, 'sp'), may hold values from -0.375 to 0.375
- value_up: bfloat16 [256, 2048], P(None, 'sp'), may hold values from -0.375 to 0.375
- out_proj: bfloat16 [2048, 2048], P('sp', 'dp'), may hold values from -0.125 to 0.125
- norm_gain: float32 [2048], replicated, may hold values from 0.1 to 1.9
- expert_gate: bfloat16 [8, 2048, 1024], P('sp'), may hold values from -0.125 to 0.125
- expert_up: bfloat16 [8, 2048, 1024], P('sp'), may hold values from -0.125 to 0.125
- expert_down: bfloat16 [8, 1024, 2048], P('sp'), may hold values from -0.1875 to 0.1875
- routes: int32 [4, 2048, 2], P('dp', 'sp'), may hold values from 0 to 7, all different within a row; in each aligned block of 256 rows (0 to 255, 256 to 511, ..., all dimensions but the last counted through in order) at most 128 rows name the same one
- route_weight: float32 [4, 2048, 2], P('dp', 'sp'), may hold values from 0.2 to 1
Outputs:
- mixed: bfloat16 [4, 2048, 2048], P('dp', 'sp')
Inputs may be any that keep to these rules, and one draw needn't show every extreme that they name: `routes`: each token names two different experts. Among the tokens of one device no expert is named more than 128 times, and in every draw some expert is named exactly 128 times by some device's tokens.
All inputs are finite; a program needn't handle non-finite values.
Results may differ from a plain program's by a relative error of at most 0.0075.
Values may be sent and summed in bfloat16 or wider, within the bound.
No kernel may reach another device: no remote copies, remote signals or barrier semaphores. Data moves between devices by JAX's collectives and lax.ppermute only.
A program may use at most 128 MiB of HBM per device.

v0:
```python
import jax
import jax.numpy as jnp
from jax import lax
from jax.sharding import PartitionSpec as P

epsilon = 1e-06
rope_base = 10000.0
masked_score = -1e30


def rotate(values, positions):
    half_width = values.shape[-1] // 2
    frequency = rope_base ** (-jnp.arange(half_width, dtype=jnp.float32) / half_width)
    angles = positions.astype(jnp.float32)[:, None] * frequency[None, :]
    cosine = jnp.cos(angles)
    sine_part = jnp.sin(angles)
    if values.ndim == 3:
        cosine = cosine[:, None, :]
        sine_part = sine_part[:, None, :]
    floats = values.astype(jnp.float32)
    first_half = floats[..., :half_width]
    second_half = floats[..., half_width:]
    turned = jnp.concatenate(
        [
            first_half * cosine - second_half * sine_part,
            second_half * cosine + first_half * sine_part,
        ],
        axis=-1,
    )
    return turned.astype(jnp.bfloat16)


def rms_scaled(values, gain):
    floats = values.astype(jnp.float32)
    return floats * lax.rsqrt(jnp.mean(floats * floats, axis=-1, keepdims=True) + epsilon) * gain


def assign_slots(route_block, experts_all, capacity):
    flat_routes = route_block.reshape(-1)
    onehot = (flat_routes[:, None] == jnp.arange(experts_all, dtype=jnp.int32)[None, :]).astype(
        jnp.int32
    )
    earlier = jnp.cumsum(onehot, axis=0) - onehot
    placed = jnp.sum(earlier * onehot, axis=1)
    return flat_routes * capacity + placed


def fill_slots(rows, slot_ids, experts_all, capacity):
    pairs = slot_ids.shape[0]
    matches = jnp.arange(experts_all * capacity, dtype=jnp.int32)[:, None] == slot_ids[None, :]
    source = (
        jnp.sum(jnp.where(matches, jnp.arange(pairs, dtype=jnp.int32)[None, :], 0), axis=1) // 2
    )
    filled = jnp.any(matches, axis=1)
    picked = jnp.take(rows, source, axis=0)
    chosen = jnp.where(filled[:, None], picked, jnp.zeros_like(picked))
    return chosen.reshape(experts_all, capacity, rows.shape[-1])


def combine_slots(returned, slot_ids, weights):
    flat_back = returned.reshape(-1, returned.shape[-1])
    picked = (
        jnp.take(flat_back, slot_ids, axis=0).astype(jnp.float32).reshape(weights.shape[0], 2, -1)
    )
    return jnp.sum(weights[:, :, None] * picked, axis=1)


def shards(
    query_nope,
    query_rope,
    latent,
    key_rope,
    resid,
    latent_gain,
    key_up,
    value_up,
    out_proj,
    norm_gain,
    expert_gate,
    expert_up,
    expert_down,
    routes,
    route_weight,
):
    tokens_here = latent.shape[1]
    sp_count = lax.axis_size("sp")
    length = tokens_here * sp_count
    block = min(512, length)
    blocks = length // block
    local_pos = lax.axis_index("sp") * tokens_here + jnp.arange(tokens_here, dtype=jnp.int32)
    latent_normed = rms_scaled(latent[0], latent_gain).astype(jnp.bfloat16)
    key_turned = rotate(key_rope[0], local_pos)
    query_turned = rotate(query_rope[0], local_pos)
    all_latent, all_keyturn = (
        lax.all_gather(latent_normed, "sp", axis=0, tiled=True),
        lax.all_gather(key_turned, "sp", axis=0, tiled=True),
    )
    query_plain, query_turn = (
        lax.all_to_all(query_nope[0], "sp", split_axis=1, concat_axis=0, tiled=True),
        lax.all_to_all(query_turned, "sp", split_axis=1, concat_axis=0, tiled=True),
    )
    heads_here = query_plain.shape[1]
    key_plain = (
        jnp.dot(all_latent, key_up, preferred_element_type=jnp.float32)
        .astype(jnp.bfloat16)
        .reshape(length, heads_here, -1)
    )
    value_heads = (
        jnp.dot(all_latent, value_up, preferred_element_type=jnp.float32)
        .astype(jnp.bfloat16)
        .reshape(length, heads_here, -1)
    )
    scale = (query_plain.shape[-1] + query_turn.shape[-1]) ** (-0.5)
    key_ids = jnp.arange(length, dtype=jnp.int32)

    def one_block(items):
        index, plain_block, turn_block = items
        scores = jnp.einsum(
            "bhd,shd->hbs", plain_block, key_plain, preferred_element_type=jnp.float32
        )
        scores = (
            scores
            + jnp.einsum("bhr,sr->hbs", turn_block, all_keyturn, preferred_element_type=jnp.float32)
        ) * scale
        row_ids = index * block + jnp.arange(block, dtype=jnp.int32)
        allowed = key_ids[None, :] <= row_ids[:, None]
        scores = jnp.where(allowed[None], scores, masked_score)
        largest = jnp.max(scores, axis=-1, keepdims=True)
        powers = jnp.exp(scores - largest)
        attend = (powers / jnp.sum(powers, axis=-1, keepdims=True)).astype(jnp.bfloat16)
        return jnp.einsum(
            "hbs,shd->bhd", attend, value_heads, preferred_element_type=jnp.float32
        ).astype(jnp.bfloat16)

    attended = lax.map(
        one_block,
        (
            jnp.arange(blocks, dtype=jnp.int32),
            query_plain.reshape(blocks, block, heads_here, -1),
            query_turn.reshape(blocks, block, heads_here, -1),
        ),
    )
    attended = attended.reshape(length, heads_here, -1)
    token_heads = lax.all_to_all(attended, "sp", split_axis=0, concat_axis=1, tiled=True)
    flat_heads = token_heads.reshape(tokens_here, -1)
    head_rows = lax.all_gather(out_proj, "dp", axis=1, tiled=True)
    projected = jnp.dot(
        flat_heads,
        lax.all_gather(head_rows, "sp", axis=0, tiled=True),
        preferred_element_type=jnp.float32,
    ).astype(jnp.bfloat16)
    after_attention = resid[0].astype(jnp.float32) + projected.astype(jnp.float32)
    normed = rms_scaled(after_attention, norm_gain).astype(jnp.bfloat16)
    experts_all = sp_count * expert_gate.shape[0]
    capacity = 4 * tokens_here // experts_all
    slot_ids = assign_slots(routes[0], experts_all, capacity)
    outgoing = fill_slots(normed, slot_ids, experts_all, capacity)
    arrived = lax.all_to_all(outgoing, "sp", split_axis=0, concat_axis=0, tiled=True)
    senders, slots_now, width = arrived.shape
    rows = arrived.reshape(senders * slots_now, width)
    gate = jnp.dot(rows, expert_gate[0], preferred_element_type=jnp.float32)
    upward = jnp.dot(rows, expert_up[0], preferred_element_type=jnp.float32)
    hidden = (jax.nn.silu(gate) * upward).astype(jnp.bfloat16)
    result = jnp.dot(hidden, expert_down[0], preferred_element_type=jnp.float32).astype(
        jnp.bfloat16
    )
    returned = lax.all_to_all(
        result.reshape(senders, slots_now, width), "sp", split_axis=0, concat_axis=0, tiled=True
    )
    routed = combine_slots(returned, slot_ids, route_weight[0])
    return (after_attention + routed).astype(jnp.bfloat16)[None]


def solution(mesh):
    return jax.shard_map(
        shards,
        mesh=mesh,
        in_specs=(
            P("dp", "sp", None, None),
            P("dp", "sp", None, None),
            P("dp", "sp", None),
            P("dp", "sp", None),
            P("dp", "sp", None),
            P(),
            P(None, "sp"),
            P(None, "sp"),
            P("sp", "dp"),
            P(),
            P("sp", None, None),
            P("sp", None, None),
            P("sp", None, None),
            P("dp", "sp", None),
            P("dp", "sp", None),
        ),
        out_specs=P("dp", "sp", None),
        check_vma=False,
    )
```

profile of v0, /device:TPU:0, one launch (start us, length us, event | category | flops | bytes accessed | tf_op | source)
XLA Modules:
  0.0 489.6 jit_solution(9054582442500225814)
XLA Ops:
  12.2 16.1 %all-gather.6.cloned.1.call-done = bf16[256,2048]{1,0:T(8,128)(2,1)} async-done(((bf16[256,512]{1,0:T(8,128)(2,1)}), bf16[256,2048]{1,0:T(8,128)(2,1)}) %all-gather.6.cloned.1.call-update) | async-done | bytes 1048592 | tf_op jit(solution)/shard_map/all_gather | solution.py:146
  29.4 5.5 %all-to-all-start.1 = ((bf16[256,16,64]{0,2,1:T(8,128)(2,1)}), bf16[256,16,64]{0,2,1:T(8,128)(2,1)S(1)}, u32[]{:S(2)}, u32[]{:S(2)}) async-start(bf16[256,16,64]{0,2,1:T(8,128)(2,1)} %pad_maximum_fusion), calls=%async_computation.1 | async-start | bytes 1048576 | tf_op jit(solution)/shard_map/all_to_all | solution.py:100
  36.2 17.7 %all-to-all-done.1 = bf16[256,16,64]{0,2,1:T(8,128)(2,1)S(1)} async-done(((bf16[256,16,64]{0,2,1:T(8,128)(2,1)}), bf16[256,16,64]{0,2,1:T(8,128)(2,1)S(1)}, u32[]{:S(2)}, u32[]{:S(2)}) %all-to-all-start.1) | async-done | bytes 524320 | tf_op jit(solution)/shard_map/all_to_all | solution.py:100
  54.0 3.6 all-to-all-start
  57.6 55.9 %all_gather.13 = bf16[2048,64]{0,1:T(8,128)(2,1)S(1)} all-gather(bf16[256,64]{0,1:T(8,128)(2,1)S(1)} %pad_maximum_fusion.1), channel_id=1, replica_groups=mesh['sp'=8,'dp'=4] {'sp'}, dimensions={0}, use_global_device_ids=true | all-gather | bytes 294912 | tf_op jit(solution)/shard_map/all_gather | solution.py:96
  115.1 2.8 convolution_convert_fusion.1
  119.5 2.4 convolution_convert_fusion
  121.9 2.3 copy.93
  124.3 73.1 %while.11 = (s32[]{:T(128)}, bf16[4,512,2,128]{3,1,0,2:T(8,128)(2,1)}, s32[4]{0:T(128)S(1)}, bf16[4,512,2,128]{3,1,0,2:T(8,128)(2,1)S(1)}, bf16[2048,2,128]{2,0,...) while((s32[]{:T(128)}, ...), condition=%wide.region_4.5_spmd.clone, body=%wide.region_1.4_spmd.clone.sunk | while | flops 1360139776 | bytes 93205688 | solution.py:135
  127.3 2.8 fusion.75
  133.3 9.1 %fusion.77 = bf16[4,512,2,128]{3,1,0,2:T(8,128)(2,1)} fusion(bf16[4,512,2,128]{3,1,0,2:T(8,128)(2,1)} %get-tuple-element.211, s32[]{:T(128)} %get-tuple-element.210, bf16[2048,2,128]{2,0,1:T(8,128)(2,1)S(1)} %copy-done.5, f32[2,512]{1,0:T(2,128)S(1)} %fusion.76, f32[2,512,2048]{2,1,0:T(8,128)} %copy-done.2), kind=kOutput, calls=%fused_computation.13.clone.1 | convolution fusion | flops 543296512 | bytes 18092544 | tf_op jit(solution)/shard_map/while/body/eval_jaxpr/hbs,shd->bhd/dot_general | solution.py:131
  145.5 2.8 fusion.75
  151.5 9.2 %fusion.77 = bf16[4,512,2,128]{3,1,0,2:T(8,128)(2,1)} fusion(bf16[4,512,2,128]{3,1,0,2:T(8,128)(2,1)} %get-tuple-element.211, s32[]{:T(128)} %get-tuple-element.210, bf16[2048,2,128]{2,0,1:T(8,128)(2,1)S(1)} %copy-done.5, f32[2,512]{1,0:T(2,128)S(1)} %fusion.76, f32[2,512,2048]{2,1,0:T(8,128)} %copy-done.2), kind=kOutput, calls=%fused_computation.13.clone.1 | convolution fusion | flops 543296512 | bytes 18092544 | tf_op jit(solution)/shard_map/while/body/eval_jaxpr/hbs,shd->bhd/dot_general | solution.py:131
  163.8 2.8 fusion.75
  169.8 9.1 %fusion.77 = bf16[4,512,2,128]{3,1,0,2:T(8,128)(2,1)} fusion(bf16[4,512,2,128]{3,1,0,2:T(8,128)(2,1)} %get-tuple-element.211, s32[]{:T(128)} %get-tuple-element.210, bf16[2048,2,128]{2,0,1:T(8,128)(2,1)S(1)} %copy-done.5, f32[2,512]{1,0:T(2,128)S(1)} %fusion.76, f32[2,512,2048]{2,1,0:T(8,128)} %copy-done.2), kind=kOutput, calls=%fused_computation.13.clone.1 | convolution fusion | flops 543296512 | bytes 18092544 | tf_op jit(solution)/shard_map/while/body/eval_jaxpr/hbs,shd->bhd/dot_general | solution.py:131
  181.9 2.8 fusion.75
  188.0 9.4 %fusion.77 = bf16[4,512,2,128]{3,1,0,2:T(8,128)(2,1)} fusion(bf16[4,512,2,128]{3,1,0,2:T(8,128)(2,1)} %get-tuple-element.211, s32[]{:T(128)} %get-tuple-element.210, bf16[2048,2,128]{2,0,1:T(8,128)(2,1)S(1)} %copy-done.5, f32[2,512]{1,0:T(2,128)S(1)} %fusion.76, f32[2,512,2048]{2,1,0:T(8,128)} %copy-done.2), kind=kOutput, calls=%fused_computation.13.clone.1 | convolution fusion | flops 543296512 | bytes 18092544 | tf_op jit(solution)/shard_map/while/body/eval_jaxpr/hbs,shd->bhd/dot_general | solution.py:131
  197.3 3.7 copy.95
  201.0 3.7 all-to-all-start.2
  207.4 28.0 %all-to-all-done.2 = bf16[2048,2,128]{2,1,0:T(2,128)(2,1)S(1)} async-done(((bf16[2048,2,128]{2,1,0:T(2,128)(2,1)}), bf16[2048,2,128]{2,1,0:T(2,128)(2,1)S(1)}, u32[]{:S(2)}, u32[]{:S(2)}) %all-to-all-start.2) | async-done | bytes 1048608 | tf_op jit(solution)/shard_map/all_to_all | solution.py:144
  236.2 6.1 %multiply_reduce_fusion.1 = (f32[256]{0:T(256)S(1)}, f32[256,2048]{1,0:T(8,128)S(1)}) fusion(bf16[256,2048]{0,1:T(8,128)(2,1)S(1)} %bitcast.150, bf16[2048,2048]{1,0:T(8,128)(2,1)} %all-gather.8.cloned.1.call-done, bf16[1,256,2048]{2,1,0:T(8,128)(2,1)} %param.21), kind=kOutput, calls=%fused_computation.42 | convolution fusion | flops 2150629120 | bytes 12583936 | tf_op jit(solution)/shard_map/dot_general | solution.py:147
  242.5 6.0 %gather_fusion = bf16[1024,2048]{1,0:T(8,128)(2,1)} fusion(bf16[256,2048]{1,0:T(8,128)(2,1)S(1)} %multiply_convert_fusion.1, s32[1024]{0:T(1024)S(1)} %broadcast_clamp_fusion), kind=kCustom, calls=%fused_computation | custom fusion | bytes 8392704 | tf_op jit(solution)/shard_map/jit(_take)/gather | solution.py:55
  248.5 2.6 select_select_fusion
  251.1 95.5 %all_to_all.55 = bf16[8,128,2048]{2,1,0:T(8,128)(2,1)S(1)} all-to-all(bf16[8,128,2048]{2,1,0:T(8,128)(2,1)S(1)} %select_select_fusion), channel_id=1, replica_groups=mesh['sp'=8,'dp'=4] {'sp'}, dimensions={0} | all-to-all | bytes 8388608 | tf_op jit(solution)/shard_map/all_to_all | solution.py:158
  346.6 4.5 fusion.20
  351.1 5.4 %multiply_convert_fusion = bf16[1024,1024]{1,0:T(8,128)(2,1)S(1)} fusion(f32[1024,1024]{1,0:T(8,128)S(1)} %fusion.20, bf16[1024,2048]{1,0:T(8,128)(2,1)S(1)} %bitcast.154, bf16[1,2048,1024]{2,1,0:T(8,128)(2,1)S(1)} %copy-done.10), kind=kOutput, calls=%fused_computation.31 | convolution fusion | flops 4301258752 | bytes 14680064 | tf_op jit(solution)/shard_map/dot_general | solution.py:161
  356.5 6.1 %fusion.24 = bf16[1024,2048]{1,0:T(8,128)(2,1)} fusion(bf16[1024,1024]{1,0:T(8,128)(2,1)S(1)} %multiply_convert_fusion, bf16[1,1024,2048]{2,1,0:T(8,128)(2,1)S(1)} %copy-done.11), kind=kOutput, calls=%fused_computation.34 | convolution fusion | flops 4297064448 | bytes 10485760 | tf_op jit(solution)/shard_map/dot_general | solution.py:164
  362.6 4.9 all-to-all-start.4
  368.4 91.0 %all-to-all-done.4 = bf16[8,128,2048]{2,1,0:T(8,128)(2,1)} async-done(((bf16[8,128,2048]{2,1,0:T(8,128)(2,1)}), bf16[8,128,2048]{2,1,0:T(8,128)(2,1)}, u32[]{:S(2)}, u32[]{:S(2)}) %all-to-all-start.4) | async-done | bytes 4194336 | tf_op jit(solution)/shard_map/all_to_all | solution.py:167
  459.4 8.0 %gather_fusion.1 = bf16[512,2048]{1,0:T(8,128)(2,1)} fusion(bf16[1024,2048]{1,0:T(8,128)(2,1)} %bitcast.33, s32[1024]{0:T(1024)S(1)} %pad_clamp_fusion), kind=kCustom, calls=%fused_computation.1 | custom fusion | bytes 4196352 | tf_op jit(solution)/shard_map/jit(_take)/gather | solution.py:63
  467.4 4.4 gather.15
  471.9 9.9 %multiply_reduce_fusion = f32[256,2048]{1,0:T(8,128)S(1)} fusion(bf16[256,2,2048]{2,1,0:T(2,128)(2,1)} %gather.15, pred[256,2]{1,0:T(8,128)(4,1)S(1)} %copy.102, f32[256,2]{1,0:T(8,128)S(1)} %copy.98), kind=kLoop, calls=%fused_computation.30 | loop fusion | flops 3670016 | bytes 4196864 | tf_op jit(solution)/shard_map/reduce_sum | solution.py:65
  (114 shorter events, 39.5 us)
Async XLA Ops:
  6.5 108.5 %copy-start = (bf16[256,256]{1,0:T(8,128)(2,1)S(1)}, bf16[256,256]{1,0:T(8,128)(2,1)}, u32[]{:S(2)}) copy-start(bf16[256,256]{1,0:T(8,128)(2,1)} %param.23) | copy-start | bytes 393220
  6.5 28.3 %copy-start.4 = (bf16[1,256,16,128]{3,2,1,0:T(8,128)(2,1)S(1)}, bf16[1,256,16,128]{3,2,1,0:T(8,128)(2,1)}, u32[]{:S(2)}) copy-start(bf16[1,256,16,128]{3,2,1,0:T(8,128)(2,1)} %param.17) | copy-start | bytes 3145732
  6.5 21.8 %all-gather.6.cloned.1.call-start = ((), (), s32[]{:S(2)}) async-start(), calls=%async_computation.6 | async-start | bytes 1310720 | tf_op jit(solution)/shard_map/all_gather | solution.py:146
  7.3 107.8 %all-gather.4.cloned.1.call-start = ((), (), s32[]{:S(2)}) async-start(), calls=%async_computation.5 | async-start | bytes 1179648 | tf_op jit(solution)/shard_map/all_gather | solution.py:95
  10.0 226.1 %all-gather.8.cloned.1.call-start = ((), (), s32[]{:S(2)}) async-start(), calls=%async_computation.7 | async-start | bytes 9437184 | tf_op jit(solution)/shard_map/all_gather | solution.py:149
  29.4 24.6 %all-to-all-start.1 = ((bf16[256,16,64]{0,2,1:T(8,128)(2,1)}), bf16[256,16,64]{0,2,1:T(8,128)(2,1)S(1)}, u32[]{:S(2)}, u32[]{:S(2)}) async-start(bf16[256,16,64]{0,2,1:T(8,128)(2,1)} %pad_maximum_fusion), calls=%async_computation.1 | async-start | bytes 1048576 | tf_op jit(solution)/shard_map/all_to_all | solution.py:100
  54.0 70.2 %all-to-all-start = ((bf16[256,16,128]{2,0,1:T(8,128)(2,1)}), bf16[256,16,128]{2,0,1:T(8,128)(2,1)S(1)}, u32[]{:S(2)}, u32[]{:S(2)}) async-start(bf16[256,16,128]{2,0,1:T(8,128)(2,1)} %bitcast.127), calls=%async_computation | async-start | bytes 2097152 | tf_op jit(solution)/shard_map/all_to_all | solution.py:99
  115.1 4.4 copy-start.3
  130.1 3.2 copy-start.2
  130.1 3.2 copy-start.5
  148.3 3.2 copy-start.2
  148.3 3.2 copy-start.5
  166.5 3.2 copy-start.2
  166.6 3.2 copy-start.5
  184.7 3.2 copy-start.2
  184.7 3.2 copy-start.5
  197.3 7.4 %copy-start.6 = (s32[1,256,2]{1,2,0:T(2,128)S(1)}, s32[1,256,2]{1,2,0:T(2,128)}, u32[]{:S(2)}) copy-start(s32[1,256,2]{1,2,0:T(2,128)} %param.30) | copy-start | bytes 6148
  201.0 34.4 %all-to-all-start.2 = ((bf16[2048,2,128]{2,1,0:T(2,128)(2,1)}), bf16[2048,2,128]{2,1,0:T(2,128)(2,1)S(1)}, u32[]{:S(2)}, u32[]{:S(2)}) async-start(bf16[2048,2,128]{2,1,0:T(2,128)(2,1)} %copy.95), calls=%async_computation.2 | async-start | bytes 2097152 | tf_op jit(solution)/shard_map/all_to_all | solution.py:144
  236.1 6.1 %copy-start.7 = (f32[2048]{0:T(1024)S(1)}, f32[2048]{0:T(1024)}, u32[]{:S(2)}) copy-start(f32[2048]{0:T(1024)} %param.26) | copy-start | bytes 24580
  251.1 95.5 %copy-start.9 = (bf16[1,2048,1024]{2,1,0:T(8,128)(2,1)S(1)}, bf16[1,2048,1024]{2,1,0:T(8,128)(2,1)}, u32[]{:S(2)}) copy-start(bf16[1,2048,1024]{2,1,0:T(8,128)(2,1)} %param.28) | copy-start | bytes 12582916
  346.6 4.5 copy-start.10
  351.1 5.4 %copy-start.11 = (bf16[1,1024,2048]{2,1,0:T(8,128)(2,1)S(1)}, bf16[1,1024,2048]{2,1,0:T(8,128)(2,1)}, u32[]{:S(2)}) copy-start(bf16[1,1024,2048]{2,1,0:T(8,128)(2,1)} %param.29) | copy-start | bytes 12582916
  362.6 5.6 %copy-start.8 = (f32[1,256,2]{1,2,0:T(2,128)S(1)}, f32[1,256,2]{1,2,0:T(2,128)}, u32[]{:S(2)}) copy-start(f32[1,256,2]{1,2,0:T(2,128)} %param.31) | copy-start | bytes 6148
  362.6 96.9 %all-to-all-start.4 = ((bf16[8,128,2048]{2,1,0:T(8,128)(2,1)}), bf16[8,128,2048]{2,1,0:T(8,128)(2,1)}, u32[]{:S(2)}, u32[]{:S(2)}) async-start(bf16[8,128,2048]{2,1,0:T(8,128)(2,1)} %bitcast.152), calls=%async_computation.4 | async-start | bytes 8388608 | tf_op jit(solution)/shard_map/all_to_all | solution.py:167
  467.4 15.6 %copy-start.1 = (bf16[256,256]{1,0:T(8,128)(2,1)S(1)}, bf16[256,256]{1,0:T(8,128)(2,1)}, u32[]{:S(2)}) copy-start(bf16[256,256]{1,0:T(8,128)(2,1)} %param.23) | copy-start | bytes 393220
Sparse Core Ops, SparseCore 0:
  8.9 19.4 all-gather.5
  30.5 57.7 all-gather.3
  90.4 131.3 all-gather.7
where the time goes:
time: 490 us
  waiting for transfers between devices  154 us (31%)
  blocking collectives  151 us (31%)
  matrix products  80.1 us (16%)
  local copies, waits for them, and re-layouts  40 us (8%)
  other arithmetic  30.5 us (6%)
  starting transfers between devices  17.9 us (4%)
  between operations  13.5 us (3%)
    all_to_all x1, blocking collectives, shards(): lax.all_to_all(outgoing, 'sp', split_axis=0, concat_axis=0, tiled=True)  95.5 us
    all_to_all x1, waiting for transfers between devices, shards(): lax.all_to_all(result.reshape(senders, slots_now, width), 'sp', split_axi...  91 us
    all_gather x1, blocking collectives, shards(): lax.all_gather(key_turned, 'sp', axis=0, tiled=True)  55.9 us
    dot_general x4, matrix products, one_block(): jnp.einsum('hbs,shd->bhd', attend, value_heads, preferred_element_type=jn...  36.8 us
    all_to_all x1, waiting for transfers between devices, shards(): lax.all_to_all(attended, 'sp', split_axis=0, concat_axis=1, tiled=True)  28 us
    all_to_all x1, waiting for transfers between devices, shards(): lax.all_to_all(query_turned, 'sp', split_axis=1, concat_axis=0, tiled=True)  17.7 us
    all_gather x1, waiting for transfers between devices, shards(): head_rows = lax.all_gather(out_proj, 'dp', axis=1, tiled=True)  16.1 us
    gather x2, local copies, waits for them, and re-layouts, combine_slots(): jnp.take(flat_back, slot_ids, axis=0).astype(jnp.float32)  12.4 us
  transfers between devices with their start and end apart: 7, of which 4 were waited for; matrix products, arithmetic and copies ran while one was open for 18% of the time, Pallas kernels for 0%

commit v1 on v0

--- a/solution.py
+++ b/solution.py
@@ -141,7 +141,15 @@
         ),
     )
     attended = attended.reshape(length, heads_here, -1)
-    token_heads = lax.all_to_all(attended, "sp", split_axis=0, concat_axis=1, tiled=True)
+    ways, here = (lax.axis_size("sp"), lax.axis_index("sp"))
+    width_2 = attended.shape[0] // ways
+    turned_2 = jnp.roll(attended, -here * width_2, axis=0)
+    got = [lax.slice_in_dim(turned_2, 0, width_2, axis=0)]
+    for far in range(1, ways):
+        sent = lax.slice_in_dim(turned_2, far * width_2, (far + 1) * width_2, axis=0)
+        got.append(lax.ppermute(sent, "sp", [(d, (d + far) % ways) for d in range(ways)]))
+    line = jnp.concatenate(got[::-1], axis=1)
+    token_heads = jnp.roll(line, (here + 1) * got[0].shape[1], axis=1)
     flat_heads = token_heads.reshape(tokens_here, -1)
     head_rows = lax.all_gather(out_proj, "dp", axis=1, tiled=True)
     projected = jnp.dot(

time: 490 us -> 482 us (0.984)
  waiting for transfers between devices: 154 us -> 141 us
    ppermute x0 -> x7, waiting for transfers between devices: none -> 38.2 us  [shards(): lax.ppermute(sent, 'sp', [(d, (d + far) % ways) for d in range(ways)])]
    all_to_all x1 -> x0, waiting for transfers between devices: 28 us -> none  [shards(): lax.all_to_all(attended, 'sp', split_axis=0, concat_axis=1, tiled=True)]
    all_gather x1, waiting for transfers between devices: 16.1 us -> 4.54 us  [shards(): head_rows = lax.all_gather(out_proj, 'dp', axis=1, tiled=True)]
    all_to_all x1, waiting for transfers between devices: 17.7 us -> 6.58 us  [shards(): lax.all_to_all(query_turned, 'sp', split_axis=1, concat_axis=0, tiled=True)]
    ppermute x0 -> x7, starting transfers between devices: none -> 6.34 us  [shards(): lax.ppermute(sent, 'sp', [(d, (d + far) % ways) for d in range(ways)])]
  transfers between devices with their start and end apart: 7 -> 13, of which waited for: 4 -> 8; matrix products, arithmetic and copies ran while one was open for 18% -> 18% of each run, Pallas kernels for 0% -> 0%
where the time goes in v1:
time: 482 us; the launch traced here: 481 us
  blocking collectives  151 us (31%)
  waiting for transfers between devices  141 us (29%)
  matrix products  79.9 us (17%)
  local copies, waits for them, and re-layouts  37.7 us (8%)
  other arithmetic  32.4 us (7%)
  starting transfers between devices  22.3 us (5%)
  between operations  13.7 us (3%)
    all_to_all x1, blocking collectives, shards(): lax.all_to_all(outgoing, 'sp', split_axis=0, concat_axis=0, tiled=True)  95.2 us
    all_to_all x1, waiting for transfers between devices, shards(): lax.all_to_all(result.reshape(senders, slots_now, width), 'sp', split_axi...  91 us
    all_gather x1, blocking collectives, shards(): lax.all_gather(key_turned, 'sp', axis=0, tiled=True)  55.6 us
    ppermute x7, waiting for transfers between devices, shards(): lax.ppermute(sent, 'sp', [(d, (d + far) % ways) for d in range(ways)])  38.2 us
    dot_general x4, matrix products, one_block(): jnp.einsum('hbs,shd->bhd', attend, value_heads, preferred_element_type=jn...  36.6 us
    gather x2, local copies, waits for them, and re-layouts, combine_slots(): jnp.take(flat_back, slot_ids, axis=0).astype(jnp.float32)  12.4 us
    dot_general x4, matrix products, one_block(): jnp.einsum('bhr,sr->hbs', turn_block, all_keyturn, preferred_element_type...  11.1 us
    reduce_sum x1, other arithmetic, combine_slots(): return jnp.sum(weights[:, :, None] * picked, axis=1)  9.9 us
  transfers between devices with their start and end apart: 13, of which 8 were waited for; matrix products, arithmetic and copies ran while one was open for 18% of the time, Pallas kernels for 0%

profile of v1, /device:TPU:0, one launch (start us, length us, event | category | flops | bytes accessed | tf_op | source)
XLA Modules:
  0.0 480.6 jit_solution(2635150875767537805)
XLA Ops:
  13.2 7.3 %all-to-all-start.1 = ((bf16[256,16,64]{0,2,1:T(8,128)(2,1)}), bf16[256,16,64]{0,2,1:T(8,128)(2,1)S(1)}, u32[]{:S(2)}, u32[]{:S(2)}) async-start(bf16[256,16,64]{0,2,1:T(8,128)(2,1)} %pad_maximum_fusion), calls=%async_computation.1 | async-start | bytes 1048576 | tf_op jit(solution)/shard_map/all_to_all | solution.py:100
  23.8 4.5 all-gather.6.cloned.1.call-done
  28.5 6.6 %all-to-all-done.1 = bf16[256,16,64]{0,2,1:T(8,128)(2,1)S(1)} async-done(((bf16[256,16,64]{0,2,1:T(8,128)(2,1)}), bf16[256,16,64]{0,2,1:T(8,128)(2,1)S(1)}, u32[]{:S(2)}, u32[]{:S(2)}) %all-to-all-start.1) | async-done | bytes 524320 | tf_op jit(solution)/shard_map/all_to_all | solution.py:100
  35.0 3.6 all-to-all-start
  38.7 55.6 %all_gather.13 = bf16[2048,64]{0,1:T(8,128)(2,1)S(1)} all-gather(bf16[256,64]{0,1:T(8,128)(2,1)S(1)} %pad_maximum_fusion.1), channel_id=1, replica_groups=mesh['sp'=8,'dp'=4] {'sp'}, dimensions={0}, use_global_device_ids=true | all-gather | bytes 294912 | tf_op jit(solution)/shard_map/all_gather | solution.py:96
  96.2 2.8 convolution_convert_fusion.1
  105.4 74.3 %while.11 = (s32[]{:T(128)}, bf16[4,512,2,128]{3,1,0,2:T(8,128)(2,1)}, s32[4]{0:T(128)S(1)}, bf16[4,512,2,128]{3,1,0,2:T(8,128)(2,1)S(1)}, bf16[2048,2,128]{2,0,...) while((s32[]{:T(128)}, ...), condition=%wide.region_4.5_spmd.clone, body=%wide.region_1.4_spmd.clone.sunk | while | flops 1360139776 | bytes 93205688 | solution.py:135
  108.6 2.8 fusion.77
  114.6 9.2 %fusion.79 = bf16[4,512,2,128]{3,1,0,2:T(8,128)(2,1)} fusion(bf16[4,512,2,128]{3,1,0,2:T(8,128)(2,1)} %get-tuple-element.202, s32[]{:T(128)} %get-tuple-element.201, bf16[2048,2,128]{2,0,1:T(8,128)(2,1)S(1)} %copy-done.5, f32[2,512]{1,0:T(2,128)S(1)} %fusion.78, f32[2,512,2048]{2,1,0:T(8,128)} %copy-done.2), kind=kOutput, calls=%fused_computation.13.clone.1 | convolution fusion | flops 543296512 | bytes 18092544 | tf_op jit(solution)/shard_map/while/body/eval_jaxpr/hbs,shd->bhd/dot_general | solution.py:131
  127.0 2.8 fusion.77
  133.8 9.3 %fusion.79 = bf16[4,512,2,128]{3,1,0,2:T(8,128)(2,1)} fusion(bf16[4,512,2,128]{3,1,0,2:T(8,128)(2,1)} %get-tuple-element.202, s32[]{:T(128)} %get-tuple-element.201, bf16[2048,2,128]{2,0,1:T(8,128)(2,1)S(1)} %copy-done.5, f32[2,512]{1,0:T(2,128)S(1)} %fusion.78, f32[2,512,2048]{2,1,0:T(8,128)} %copy-done.2), kind=kOutput, calls=%fused_computation.13.clone.1 | convolution fusion | flops 543296512 | bytes 18092544 | tf_op jit(solution)/shard_map/while/body/eval_jaxpr/hbs,shd->bhd/dot_general | solution.py:131
  146.3 2.8 fusion.77
  152.3 9.1 %fusion.79 = bf16[4,512,2,128]{3,1,0,2:T(8,128)(2,1)} fusion(bf16[4,512,2,128]{3,1,0,2:T(8,128)(2,1)} %get-tuple-element.202, s32[]{:T(128)} %get-tuple-element.201, bf16[2048,2,128]{2,0,1:T(8,128)(2,1)S(1)} %copy-done.5, f32[2,512]{1,0:T(2,128)S(1)} %fusion.78, f32[2,512,2048]{2,1,0:T(8,128)} %copy-done.2), kind=kOutput, calls=%fused_computation.13.clone.1 | convolution fusion | flops 543296512 | bytes 18092544 | tf_op jit(solution)/shard_map/while/body/eval_jaxpr/hbs,shd->bhd/dot_general | solution.py:131
  164.6 2.8 fusion.77
  170.6 9.1 %fusion.79 = bf16[4,512,2,128]{3,1,0,2:T(8,128)(2,1)} fusion(bf16[4,512,2,128]{3,1,0,2:T(8,128)(2,1)} %get-tuple-element.202, s32[]{:T(128)} %get-tuple-element.201, bf16[2048,2,128]{2,0,1:T(8,128)(2,1)S(1)} %copy-done.5, f32[2,512]{1,0:T(2,128)S(1)} %fusion.78, f32[2,512,2048]{2,1,0:T(8,128)} %copy-done.2), kind=kOutput, calls=%fused_computation.13.clone.1 | convolution fusion | flops 543296512 | bytes 18092544 | tf_op jit(solution)/shard_map/while/body/eval_jaxpr/hbs,shd->bhd/dot_general | solution.py:131
  181.6 2.6 collective-permute-start
  184.5 3.0 collective-permute-start.3
  187.7 3.1 collective-permute-done
  190.9 7.0 %collective-permute-done.1 = bf16[256,2,128]{2,0,1:T(8,128)(2,1)S(1)} collective-permute-done((bf16[256,2,128]{2,0,1:T(8,128)(2,1)S(1)}, bf16[256,2,128]{2,0,1:T(8,128)(2,1)S(1)}, u32[]{:S(2)}, u32[]{:S(2)}) %collective-permute-start.1) | collective-permute-done | bytes 131104 | tf_op jit(solution)/shard_map/ppermute | solution.py:150
  198.5 3.6 collective-permute-done.2
  202.1 23.3 %collective-permute-done.3 = bf16[256,2,128]{2,0,1:T(8,128)(2,1)S(1)} collective-permute-done((bf16[256,2,128]{2,0,1:T(8,128)(2,1)S(1)}, bf16[256,2,128]{2,0,1:T(8,128)(2,1)S(1)}, u32[]{:S(2)}, u32[]{:S(2)}) %collective-permute-start.3) | collective-permute-done | bytes 131104 | tf_op jit(solution)/shard_map/ppermute | solution.py:150
  227.6 6.1 %multiply_reduce_fusion.1 = (f32[256]{0:T(256)S(1)}, f32[256,2048]{1,0:T(8,128)S(1)}) fusion(bf16[256,2048]{0,1:T(8,128)(2,1)S(1)} %bitcast.147, bf16[2048,2048]{1,0:T(8,128)(2,1)} %all-gather.8.cloned.1.call-done, bf16[1,256,2048]{2,1,0:T(8,128)(2,1)} %param.21), kind=kOutput, calls=%fused_computation.44 | convolution fusion | flops 2150629120 | bytes 12583936 | tf_op jit(solution)/shard_map/dot_general | solution.py:155
  233.9 6.0 %gather_fusion = bf16[1024,2048]{1,0:T(8,128)(2,1)} fusion(bf16[256,2048]{1,0:T(8,128)(2,1)S(1)} %multiply_convert_fusion.1, s32[1024]{0:T(1024)S(1)} %broadcast_clamp_fusion), kind=kCustom, calls=%fused_computation | custom fusion | bytes 8392704 | tf_op jit(solution)/shard_map/jit(_take)/gather | solution.py:55
  242.5 95.2 %all_to_all.40 = bf16[8,128,2048]{2,1,0:T(8,128)(2,1)S(1)} all-to-all(bf16[8,128,2048]{2,1,0:T(8,128)(2,1)S(1)} %select_select_fusion), channel_id=1, replica_groups=mesh['sp'=8,'dp'=4] {'sp'}, dimensions={0} | all-to-all | bytes 8388608 | tf_op jit(solution)/shard_map/all_to_all | solution.py:166
  337.7 4.5 fusion.20
  342.2 5.4 %multiply_convert_fusion = bf16[1024,1024]{1,0:T(8,128)(2,1)S(1)} fusion(f32[1024,1024]{1,0:T(8,128)S(1)} %fusion.20, bf16[1024,2048]{1,0:T(8,128)(2,1)S(1)} %bitcast.151, bf16[1,2048,1024]{2,1,0:T(8,128)(2,1)S(1)} %copy-done.13), kind=kOutput, calls=%fused_computation.31 | convolution fusion | flops 4301258752 | bytes 14680064 | tf_op jit(solution)/shard_map/dot_general | solution.py:169
  347.6 6.1 %fusion.24 = bf16[1024,2048]{1,0:T(8,128)(2,1)} fusion(bf16[1024,1024]{1,0:T(8,128)(2,1)S(1)} %multiply_convert_fusion, bf16[1,1024,2048]{2,1,0:T(8,128)(2,1)S(1)} %copy-done.14), kind=kOutput, calls=%fused_computation.34 | convolution fusion | flops 4297064448 | bytes 10485760 | tf_op jit(solution)/shard_map/dot_general | solution.py:172
  353.7 4.9 %all-to-all-start.3 = ((bf16[8,128,2048]{2,1,0:T(8,128)(2,1)}), bf16[8,128,2048]{2,1,0:T(8,128)(2,1)}, u32[]{:S(2)}, u32[]{:S(2)}) async-start(bf16[8,128,2048]{2,1,0:T(8,128)(2,1)} %bitcast.149), calls=%async_computation.3 | async-start | bytes 8388608 | tf_op jit(solution)/shard_map/all_to_all | solution.py:175
  359.5 91.0 %all-to-all-done.3 = bf16[8,128,2048]{2,1,0:T(8,128)(2,1)} async-done(((bf16[8,128,2048]{2,1,0:T(8,128)(2,1)}), bf16[8,128,2048]{2,1,0:T(8,128)(2,1)}, u32[]{:S(2)}, u32[]{:S(2)}) %all-to-all-start.3) | async-done | bytes 4194336 | tf_op jit(solution)/shard_map/all_to_all | solution.py:175
  450.5 8.0 %gather_fusion.1 = bf16[512,2048]{1,0:T(8,128)(2,1)} fusion(bf16[1024,2048]{1,0:T(8,128)(2,1)} %bitcast.31, s32[1024]{0:T(1024)S(1)} %pad_clamp_fusion), kind=kCustom, calls=%fused_computation.1 | custom fusion | bytes 4196352 | tf_op jit(solution)/shard_map/jit(_take)/gather | solution.py:63
  458.5 4.4 gather.15
  462.9 9.9 %multiply_reduce_fusion = f32[256,2048]{1,0:T(8,128)S(1)} fusion(bf16[256,2,2048]{2,1,0:T(2,128)(2,1)} %gather.15, pred[256,2]{1,0:T(8,128)(4,1)S(1)} %copy.69, f32[256,2]{1,0:T(8,128)S(1)} %copy.65), kind=kLoop, calls=%fused_computation.30 | loop fusion | flops 3670016 | bytes 4196864 | tf_op jit(solution)/shard_map/reduce_sum | solution.py:65
  (149 shorter events, 51.9 us)
Async XLA Ops:
  6.5 89.7 %copy-start = (bf16[256,256]{1,0:T(8,128)(2,1)S(1)}, bf16[256,256]{1,0:T(8,128)(2,1)}, u32[]{:S(2)}) copy-start(bf16[256,256]{1,0:T(8,128)(2,1)} %param.23) | copy-start | bytes 393220
  6.5 21.8 %all-gather.6.cloned.1.call-start = ((), (), s32[]{:S(2)}) async-start(), calls=%async_computation.5 | async-start | bytes 1310720 | tf_op jit(solution)/shard_map/all_gather | solution.py:154
  7.3 89.0 %all-gather.4.cloned.1.call-start = ((), (), s32[]{:S(2)}) async-start(), calls=%async_computation.4 | async-start | bytes 1179648 | tf_op jit(solution)/shard_map/all_gather | solution.py:95
  12.2 8.4 %copy-start.8 = (s32[1,256,2]{1,2,0:T(2,128)S(1)}, s32[1,256,2]{1,2,0:T(2,128)}, u32[]{:S(2)}) copy-start(s32[1,256,2]{1,2,0:T(2,128)} %param.30) | copy-start | bytes 6148
  12.2 8.9 %copy-start.4 = (bf16[1,256,16,128]{3,2,1,0:T(8,128)(2,1)S(1)}, bf16[1,256,16,128]{3,2,1,0:T(8,128)(2,1)}, u32[]{:S(2)}) copy-start(bf16[1,256,16,128]{3,2,1,0:T(8,128)(2,1)} %param.17) | copy-start | bytes 3145732
  13.2 21.8 %all-to-all-start.1 = ((bf16[256,16,64]{0,2,1:T(8,128)(2,1)}), bf16[256,16,64]{0,2,1:T(8,128)(2,1)S(1)}, u32[]{:S(2)}, u32[]{:S(2)}) async-start(bf16[256,16,64]{0,2,1:T(8,128)(2,1)} %pad_maximum_fusion), calls=%async_computation.1 | async-start | bytes 1048576 | tf_op jit(solution)/shard_map/all_to_all | solution.py:100
  20.6 207.0 %all-gather.8.cloned.1.call-start = ((), (), s32[]{:S(2)}) async-start(), calls=%async_computation.6 | async-start | bytes 9437184 | tf_op jit(solution)/shard_map/all_gather | solution.py:157
  28.5 66.2 %copy-start.6 = (s32[512]{0:T(512)}, s32[512]{0:T(512)S(1)}, u32[]{:S(2)}) copy-start(s32[512]{0:T(512)S(1)} %fusion.38) | copy-start | bytes 6148
  35.0 70.3 %all-to-all-start = ((bf16[256,16,128]{2,0,1:T(8,128)(2,1)}), bf16[256,16,128]{2,0,1:T(8,128)(2,1)S(1)}, u32[]{:S(2)}, u32[]{:S(2)}) async-start(bf16[256,16,128]{2,0,1:T(8,128)(2,1)} %bitcast.124), calls=%async_computation | async-start | bytes 2097152 | tf_op jit(solution)/shard_map/all_to_all | solution.py:99
  96.2 4.4 copy-start.3
  111.4 3.2 copy-start.2
  129.8 4.1 copy-start.2
  129.8 4.1 copy-start.5
  149.1 3.2 copy-start.2
  167.3 3.2 copy-start.2
  167.4 3.2 copy-start.5
  181.6 9.3 %collective-permute-start = (bf16[256,2,128]{2,0,1:T(8,128)(2,1)S(1)}, bf16[256,2,128]{2,0,1:T(8,128)(2,1)S(1)}, u32[]{:S(2)}, u32[]{:S(2)}) collective-permute-start(bf16[256,2,128]{2,0,1:T(8,128)(2,1)S(1)} %get-tuple-element.135), channel_id=1, source_target_pairs={{0,28},{4,0},{8,4},{12,8},{16,12},{20,16},{24,20},{28,24},{1,29},{... | collective-permute-start | bytes 393224 | tf_op jit(solution)/shard_map/ppermute | solution.py:150
  184.2 13.8 %collective-permute-start.1 = (bf16[256,2,128]{2,0,1:T(8,128)(2,1)S(1)}, bf16[256,2,128]{2,0,1:T(8,128)(2,1)S(1)}, u32[]{:S(2)}, u32[]{:S(2)}) collective-permute-start(bf16[256,2,128]{2,0,1:T(8,128)(2,1)S(1)} %get-tuple-element.134), channel_id=1, source_target_pairs={{0,24},{4,28},{8,0},{12,4},{16,8},{20,12},{24,16},{28,20},{1,25},{... | collective-permute-start | bytes 393224 | tf_op jit(solution)/shard_map/ppermute | solution.py:150
  184.5 17.6 %collective-permute-start.2 = (bf16[256,2,128]{2,0,1:T(8,128)(2,1)S(1)}, bf16[256,2,128]{2,0,1:T(8,128)(2,1)S(1)}, u32[]{:S(2)}, u32[]{:S(2)}) collective-permute-start(bf16[256,2,128]{2,0,1:T(8,128)(2,1)S(1)} %get-tuple-element.133), channel_id=1, source_target_pairs={{0,20},{4,24},{8,28},{12,0},{16,4},{20,8},{24,12},{28,16},{1,21},{... | collective-permute-start | bytes 393224 | tf_op jit(solution)/shard_map/ppermute | solution.py:150
  184.5 40.9 %collective-permute-start.3 = (bf16[256,2,128]{2,0,1:T(8,128)(2,1)S(1)}, bf16[256,2,128]{2,0,1:T(8,128)(2,1)S(1)}, u32[]{:S(2)}, u32[]{:S(2)}) collective-permute-start(bf16[256,2,128]{2,0,1:T(8,128)(2,1)S(1)} %get-tuple-element.132), channel_id=1, source_target_pairs={{0,16},{4,20},{8,24},{12,28},{16,0},{20,4},{24,8},{28,12},{1,17},{... | collective-permute-start | bytes 393224 | tf_op jit(solution)/shard_map/ppermute | solution.py:150
  187.5 39.0 %collective-permute-start.4 = (bf16[256,2,128]{2,0,1:T(8,128)(2,1)S(1)}, bf16[256,2,128]{2,0,1:T(8,128)(2,1)S(1)}, u32[]{:S(2)}, u32[]{:S(2)}) collective-permute-start(bf16[256,2,128]{2,0,1:T(8,128)(2,1)S(1)} %get-tuple-element.131), channel_id=1, source_target_pairs={{0,12},{4,16},{8,20},{12,24},{16,28},{20,0},{24,4},{28,8},{1,13},{... | collective-permute-start | bytes 393224 | tf_op jit(solution)/shard_map/ppermute | solution.py:150
  190.9 35.7 %collective-permute-start.5 = (bf16[256,2,128]{2,0,1:T(8,128)(2,1)S(1)}, bf16[256,2,128]{2,0,1:T(8,128)(2,1)S(1)}, u32[]{:S(2)}, u32[]{:S(2)}) collective-permute-start(bf16[256,2,128]{2,0,1:T(8,128)(2,1)S(1)} %get-tuple-element.130), channel_id=1, source_target_pairs={{0,8},{4,12},{8,16},{12,20},{16,24},{20,28},{24,0},{28,4},{1,9},{5... | collective-permute-start | bytes 393224 | tf_op jit(solution)/shard_map/ppermute | solution.py:150
  197.9 28.7 %collective-permute-start.6 = (bf16[256,2,128]{2,0,1:T(8,128)(2,1)S(1)}, bf16[256,2,128]{2,0,1:T(8,128)(2,1)S(1)}, u32[]{:S(2)}, u32[]{:S(2)}) collective-permute-start(bf16[256,2,128]{2,0,1:T(8,128)(2,1)S(1)} %get-tuple-element.129), channel_id=1, source_target_pairs={{0,4},{4,8},{8,12},{12,16},{16,20},{20,24},{24,28},{28,0},{1,5},{5... | collective-permute-start | bytes 393224 | tf_op jit(solution)/shard_map/ppermute | solution.py:150
  227.6 6.1 %copy-start.10 = (f32[2048]{0:T(1024)S(1)}, f32[2048]{0:T(1024)}, u32[]{:S(2)}) copy-start(f32[2048]{0:T(1024)} %param.26) | copy-start | bytes 24580
  242.5 95.2 %copy-start.12 = (bf16[1,2048,1024]{2,1,0:T(8,128)(2,1)S(1)}, bf16[1,2048,1024]{2,1,0:T(8,128)(2,1)}, u32[]{:S(2)}) copy-start(bf16[1,2048,1024]{2,1,0:T(8,128)(2,1)} %param.28) | copy-start | bytes 12582916
  337.7 4.5 copy-start.13
  342.2 5.4 %copy-start.14 = (bf16[1,1024,2048]{2,1,0:T(8,128)(2,1)S(1)}, bf16[1,1024,2048]{2,1,0:T(8,128)(2,1)}, u32[]{:S(2)}) copy-start(bf16[1,1024,2048]{2,1,0:T(8,128)(2,1)} %param.29) | copy-start | bytes 12582916
  353.7 4.9 %copy-start.7 = (s32[512]{0:T(512)S(1)}, s32[512]{0:T(512)}, u32[]{:S(2)}) copy-start(s32[512]{0:T(512)} %copy-done.6) | copy-start | bytes 6148
  353.7 5.1 %copy-start.9 = (s32[1,256,2]{1,2,0:T(2,128)S(1)}, s32[1,256,2]{1,2,0:T(2,128)}, u32[]{:S(2)}) copy-start(s32[1,256,2]{1,2,0:T(2,128)} %param.30) | copy-start | bytes 6148
  353.7 5.7 %copy-start.11 = (f32[1,256,2]{1,2,0:T(2,128)S(1)}, f32[1,256,2]{1,2,0:T(2,128)}, u32[]{:S(2)}) copy-start(f32[1,256,2]{1,2,0:T(2,128)} %param.31) | copy-start | bytes 6148
  353.7 96.9 %all-to-all-start.3 = ((bf16[8,128,2048]{2,1,0:T(8,128)(2,1)}), bf16[8,128,2048]{2,1,0:T(8,128)(2,1)}, u32[]{:S(2)}, u32[]{:S(2)}) async-start(bf16[8,128,2048]{2,1,0:T(8,128)(2,1)} %bitcast.149), calls=%async_computation.3 | async-start | bytes 8388608 | tf_op jit(solution)/shard_map/all_to_all | solution.py:175
  462.9 11.2 %copy-start.1 = (bf16[256,256]{1,0:T(8,128)(2,1)S(1)}, bf16[256,256]{1,0:T(8,128)(2,1)}, u32[]{:S(2)}) copy-start(bf16[256,256]{1,0:T(8,128)(2,1)} %param.23) | copy-start | bytes 393220
  (2 other events, 6.4 us)
Sparse Core Ops, SparseCore 0:
  8.9 19.4 all-gather.5
  30.5 49.5 all-gather.3
  82.2 143.7 all-gather.7
